TPU v7x, 32 devices: a whole 2x2x4 slice. The times are simulated.
32 devices in a mesh: gr: 2 (over x), sp: 8 (over z, y), tp: 2 (over core).
Axes of the slice: x: 2, y: 2, z: 4, core: 2. Of those that a mesh axis runs over, the one named last changes fastest.
Arguments:
- inputs: bfloat16 [4096, 2048], P(('gr', 'sp'), 'tp'), parts along dimension 0, may hold values from -6 to 6
- x_weight: bfloat16 [2048, 4096], P(None, 'tp'), may hold values from -0.125 to 0.125
- b_weight: bfloat16 [2048, 2048], P(None, 'tp'), may hold values from -0.125 to 0.125
- dt_weight: bfloat16 [2048, 128], replicated, may hold values from -0.125 to 0.125
- dt_bias: float32 [2, 64], replicated, may hold values from -2 to -1
- decay_rate: float32 [2, 64], replicated, may hold values from 0.3 to 10
- conv_x: bfloat16 [5, 4096], P(None, 'tp'), may hold values from -2.5 to 2.5
- conv_b: bfloat16 [5, 2048], P(None, 'tp'), may hold values from -2.5 to 2.5
- query_c: bfloat16 [2, 16, 128], P('gr', 'tp'), parts along dimension 0, may hold values from -6 to 6
- query_gate: bfloat16 [2, 64, 64], P('gr', 'tp'), parts along dimension 0, may hold values from -6 to 6
- read_span: int32 [2], P('gr'), parts along dimension 0, may hold values from 0 to 15
- read_gain: float32 [64, 64], P('tp'), may hold values from 0.1 to 1.9
Outputs:
- span_cache: bfloat16 [32, 2, 64, 8192], P('gr', None, 'tp', 'sp'), parts along dimension 0
- first_read: bfloat16 [2, 64, 64], P('gr', 'tp'), parts along dimension 0
There are 2 independent parts, one for each index of `gr`. A program takes and returns all parts, laid end to end along the dimension named above; an argument that names none is the same for every part. Nothing has to cross between parts.
Inputs may be any that keep to these rules, and one draw needn't show every extreme that they name: read_span holds one span index from 0 to 15.
All inputs are finite; a program needn't handle non-finite values.
Results may differ from a plain program's by a relative error of at most 0.009.
Values may be sent and summed in bfloat16 or wider, within the bound.
A program may use at most 64 MiB of HBM per device.

v0:
```python
import jax
import jax.numpy as jnp
from jax import lax
from jax.sharding import PartitionSpec as P

H = 64
P_SIZE = 64
G = 16
N = 128
KW = 5
SPAN = 128


EPSILON = 1e-06


def extended(shard, sides, width):
    for axis, dim in sides:
        size, length = (lax.axis_size(axis), shard.shape[dim])
        up = [(i, (i + 1) % size) for i in range(size - 1)]
        down = [(j, i) for i, j in up]
        last = lax.slice_in_dim(shard, length - width, length, axis=dim)
        initial = lax.slice_in_dim(shard, 0, width, axis=dim)
        before = lax.ppermute(last, axis, up)
        after = lax.ppermute(initial, axis, down)
        shard = jnp.concatenate([before, shard, after], axis=dim)
    return shard


def span_states(value_rows, key_rows, step_sizes, log_decay):
    running = jnp.cumsum(log_decay, axis=1)
    closing = running[:, -1]
    forward = jnp.exp(closing[:, None, 0] - running[:, :, 0]) * step_sizes[:, :, 0]
    backward = jnp.exp(running[:, :, 1] - log_decay[:, :, 1]) * step_sizes[:, :, 1]
    weights = jnp.stack([forward, backward], axis=2)
    states = jnp.einsum(
        "kseh,kshn,kshp->kehnp",
        weights,
        key_rows.astype(jnp.float32),
        value_rows.astype(jnp.float32),
    )
    return (states, closing)


def read_weights(span_logs, chosen):
    span_count = span_logs.shape[0]
    ahead_sum = jnp.cumsum(span_logs[:, 0], axis=0)
    behind = jnp.flip(jnp.cumsum(jnp.flip(span_logs[:, 1], 0), axis=0), 0)
    positions = jnp.arange(span_count, dtype=jnp.int32)[:, None]
    ahead_pick = lax.dynamic_slice_in_dim(ahead_sum, chosen, 1, 0)
    behind_pick = lax.dynamic_slice_in_dim(behind, chosen, 1, 0)
    before = positions <= chosen
    after = positions >= chosen
    forward = jnp.where(before, jnp.exp(jnp.where(before, ahead_pick - ahead_sum, 0.0)), 0.0)
    backward = jnp.where(after, jnp.exp(jnp.where(after, behind_pick - behind, 0.0)), 0.0)
    return jnp.stack([forward, backward], axis=1)


def per_device(
    inputs,
    x_weight,
    b_weight,
    dt_weight,
    dt_bias,
    decay_rate,
    conv_x,
    conv_b,
    query_c,
    query_gate,
    read_span,
    read_gain,
):
    tokens = inputs.shape[0]
    heads_local = x_weight.shape[1] // P_SIZE
    per_group = H // G
    tp_index = lax.axis_index("tp")
    sp_index = lax.axis_index("sp")
    dt_local = lax.dynamic_slice_in_dim(
        dt_weight.reshape(dt_weight.shape[0], 2, H), tp_index * heads_local, heads_local, 2
    )
    dt_local = dt_local.reshape(dt_weight.shape[0], 2 * heads_local)
    slab_piece = lax.all_gather(inputs, "tp", axis=1, tiled=True)
    x_part = jnp.dot(slab_piece, x_weight, preferred_element_type=jnp.float32)
    b_part = jnp.dot(slab_piece, b_weight, preferred_element_type=jnp.float32)
    dt_part = jnp.dot(slab_piece, dt_local, preferred_element_type=jnp.float32)
    joined = jnp.concatenate([x_part.astype(jnp.bfloat16), b_part.astype(jnp.bfloat16)], axis=1)
    reach = KW // 2
    padded = extended(joined, (("sp", 0),), reach)
    taps = jnp.concatenate([conv_x, conv_b], axis=1)
    mixed_rows = jnp.zeros(joined.shape, jnp.float32)
    for offset in range(KW):
        mixed_rows = mixed_rows + taps[offset].astype(jnp.float32) * padded[
            offset : offset + tokens
        ].astype(jnp.float32)
    mixed_rows = jax.nn.silu(mixed_rows).astype(jnp.bfloat16)
    split_at = x_weight.shape[1]
    values = mixed_rows[:, :split_at]
    key_rows = mixed_rows[:, split_at:]
    length = tokens * lax.axis_size("sp")
    bias_local = lax.dynamic_slice_in_dim(dt_bias, tp_index * heads_local, heads_local, 1)
    rate_local = lax.dynamic_slice_in_dim(decay_rate, tp_index * heads_local, heads_local, 1)
    dt_raw = dt_part.astype(jnp.bfloat16).reshape(tokens, 2, heads_local)
    step_sizes = jax.nn.softplus(dt_raw.astype(jnp.float32) + bias_local)
    log_decay = -(step_sizes * rate_local) / length
    span_count = tokens // SPAN
    value_rows = values.reshape(span_count, SPAN, heads_local, P_SIZE)
    group_keys = key_rows.reshape(span_count, SPAN, heads_local // per_group, N)
    group_keys = jnp.repeat(group_keys, per_group, axis=2)
    states, closing = span_states(
        value_rows,
        group_keys,
        step_sizes.reshape(span_count, SPAN, 2, heads_local),
        log_decay.reshape(span_count, SPAN, 2, heads_local),
    )
    local_rows = states.reshape(span_count, 2, heads_local, N * P_SIZE).astype(jnp.bfloat16)
    all_logs = lax.all_gather(closing, "sp", axis=0, tiled=True)
    weights = read_weights(all_logs, read_span[0])
    cache_rows = lax.all_to_all(local_rows, "sp", split_axis=3, concat_axis=0, tiled=True)
    columns = cache_rows.shape[3] // P_SIZE
    gathered = jnp.einsum("jeh,jehx->hx", weights, cache_rows.astype(jnp.float32)).reshape(
        heads_local, columns, P_SIZE
    )
    picked = lax.dynamic_slice_in_dim(query_c[0], sp_index * columns, columns, 1)
    query_cols = jnp.repeat(picked.astype(jnp.float32), per_group, axis=0)
    partial_read = jnp.einsum("hnp,hn->hp", gathered, query_cols)
    read_total = lax.psum(partial_read, "sp")
    gated_read = read_total * jax.nn.silu(query_gate[0].astype(jnp.float32))
    square_sum = lax.psum(jnp.sum(gated_read * gated_read), "tp")
    mean_square = square_sum / (H * P_SIZE)
    first_read = (gated_read * lax.rsqrt(mean_square + EPSILON) * read_gain)[None].astype(
        jnp.bfloat16
    )
    return (cache_rows, first_read)


def solution(mesh):
    return jax.shard_map(
        per_device,
        mesh=mesh,
        in_specs=(
            P(("gr", "sp"), "tp"),
            P(None, "tp"),
            P(None, "tp"),
            P(),
            P(),
            P(),
            P(None, "tp"),
            P(None, "tp"),
            P("gr", "tp", None),
            P("gr", "tp", None),
            P("gr"),
            P("tp", None),
        ),
        out_specs=(P("gr", None, "tp", "sp"), P("gr", "tp", None)),
        check_vma=False,
    )
```

profile of v0, /device:TPU:0, one launch (start us, length us, event | category | flops | bytes accessed | tf_op | source)
XLA Modules:
  0.0 222.9 jit_solution(17773302501208012883)
XLA Ops:
  7.2 0.7 all-gather.3.cloned.1.call-update
  7.9 0.8 constant_dynamic-update-slice_fusion.1
  8.7 0.8 constant_dynamic-slice_fusion.2
  9.4 1.2 copy.63
  10.7 0.7 constant_dynamic-update-slice_fusion
  11.5 9.8 %all-gather.3.cloned.1.call-done = bf16[256,2048]{1,0:T(8,128)(2,1)} async-done(((bf16[256,1024]{1,0:T(8,128)(2,1)}), bf16[256,2048]{1,0:T(8,128)(2,1)}) %all-gather.3.cloned.1.call-update) | async-done | bytes 1048592 | tf_op jit(solution)/shard_map/all_gather | solution.py:82
  21.3 1.8 fusion.9
  23.2 0.2 copy.65
  23.5 0.2 fusion.24
  23.9 5.9 %convolution_convert_fusion = bf16[256,2048]{1,0:T(8,128)(2,1)S(1)} fusion(bf16[256,2048]{1,0:T(8,128)(2,1)S(1)} %copy-done.1, bf16[2048,2048]{1,0:T(8,128)(2,1)} %param.13), kind=kOutput, calls=%fused_computation.3 | convolution fusion | flops 2148007936 | bytes 10485760 | tf_op jit(solution)/shard_map/dot_general | solution.py:83
  29.8 1.3 convolution_convert_fusion.1
  31.1 3.6 %collective-permute-start = (bf16[2,3072]{1,0:T(2,128)(2,1)S(1)}, bf16[2,3072]{1,0:T(2,128)(2,1)S(1)}, u32[]{:S(2)}, u32[]{:S(2)}) collective-permute-start(bf16[2,3072]{1,0:T(2,128)(2,1)S(1)} %get-tuple-element.6), channel_id=1, source_target_pairs={{0,2},{2,4},{4,6},{6,8},{8,10},{10,12},{12,14},{1,3},{3,5},{5,7},{... | collective-permute-start | bytes 36872 | tf_op jit(solution)/shard_map/ppermute | solution.py:24
  34.8 1.3 collective-permute-start.1
  36.3 4.1 %collective-permute-done.1 = bf16[2,3072]{1,0:T(2,128)(2,1)S(1)} collective-permute-done((bf16[2,3072]{1,0:T(2,128)(2,1)S(1)}, bf16[2,3072]{1,0:T(2,128)(2,1)S(1)}, u32[]{:S(2)}, u32[]{:S(2)}) %collective-permute-start.1) | collective-permute-done | bytes 12320 | tf_op jit(solution)/shard_map/ppermute | solution.py:25
  40.4 0.5 maximum_maximum_fusion
  40.9 2.9 %multiply_convert_fusion = bf16[256,3072]{1,0:T(8,128)(2,1)S(1)} fusion(bf16[256,1024]{1,0:T(8,128)(2,1)S(1)} %convolution_convert_fusion.1, bf16[256,2048]{1,0:T(8,128)(2,1)S(1)} %convolution_convert_fusion, bf16[258,3072]{1,0:T(8,128)(2,1)S(1)} %get-tuple-element.5, bf16[258,3072]{1,0:T(8,128)(2,1)S(1)} %get-tuple-element.4, f32[3072]{0:T(1024)S(1)} %bitcast.103, ...), kind=kLoop, calls=%fused_computation.2 | loop fusion | flops 17301504 | bytes 9498624 | tf_op jit(solution)/shard_map/convert_element_type | solution.py:95
  43.7 0.2 slice_convert_fusion
  44.0 3.0 %reshape.152 = f32[2,128,32,64]{3,2,1,0:T(8,128)} reshape(f32[256,2048]{1,0:T(8,128)S(1)} %slice_convert_fusion) | data formatting | bytes 4194304 | tf_op jit(solution)/shard_map/convert.7
  47.0 3.8 %copy.62 = f32[2,128,32,64]{1,3,2,0:T(8,128)S(1)} copy(f32[2,128,32,64]{3,2,1,0:T(8,128)} %reshape.152) | data formatting | bytes 4194304 | tf_op jit(solution)/shard_map/convert.7
  51.0 0.6 broadcast_in_dim.43
  51.6 2.0 convert_bitcast_fusion
  53.6 14.1 %copy.82 = bf16[2,2,32,128,64]{2,1,0,4,3:T(2,128)(2,1)} copy(bf16[2,2,32,128,64]{3,4,1,2,0:T(8,128)(2,1)} %convert_bitcast_fusion) | data formatting | bytes 4194304 | tf_op jit(solution)/shard_map/convert_element_type | solution.py:115
  67.7 11.2 %reshape.153 = bf16[8,2,65536]{2,1,0:T(2,128)(2,1)} reshape(bf16[8192,2,2,32]{3,2,1,0:T(2,128)(2,1)} %bitcast.92) | data formatting | bytes 4194304
  78.9 5.6 %all-to-all-start = ((bf16[8,2,65536]{2,1,0:T(2,128)(2,1)}), bf16[8,2,65536]{2,1,0:T(2,128)(2,1)S(1)}, u32[]{:S(2)}, u32[]{:S(2)}) async-start(bf16[8,2,65536]{2,1,0:T(2,128)(2,1)} %reshape.153), calls=%async_computation | async-start | bytes 4194304 | tf_op jit(solution)/shard_map/all_to_all | solution.py:118
  85.2 65.2 %all-gather = f32[16,1,2,32]{3,2,1,0:T(2,128)S(1)} all-gather(f32[2,1,2,32]{3,2,1,0:T(2,128)S(1)} %get-tuple-element.8), channel_id=2, replica_groups=mesh['gr'=2,'sp'=8,'tp'=2] {'sp'}, dimensions={0}, use_global_device_ids=true | all-gather | bytes 4608 | tf_op jit(solution)/shard_map/all_gather | solution.py:116
  150.8 6.6 %reshape.154 = bf16[8192,2,2,32]{3,2,1,0:T(2,128)(2,1)} reshape(bf16[8,2,65536]{2,1,0:T(2,128)(2,1)S(1)} %all-to-all-done) | data formatting | bytes 4194304
  157.4 17.8 %copy.84 = bf16[2,2,32,8,1024]{4,2,1,0,3:T(8,128)(2,1)S(1)} copy(bf16[2,2,32,8,1024]{2,1,0,4,3:T(2,128)(2,1)} %bitcast.93) | data formatting | bytes 4194304 | tf_op jit(solution)/shard_map/all_to_all | solution.py:118
  175.2 2.4 %fusion.2 = bf16[32,1,1024,1]{2,1,3,0:T(2,128)(2,1)S(1)} fusion(bf16[16,2,32,1]{0,3,1,2:T(2,128)(2,1)S(1)} %copy.75, bf16[16,2,32,1024]{3,2,1,0:T(8,128)(2,1)S(1)} %bitcast.95), kind=kOutput, calls=%fused_computation.7 | convolution fusion | flops 2097152 | bytes 2164736 | tf_op jit(solution)/shard_map/jeh,jehx->hx/dot_general | solution.py:120
  178.0 33.1 %psum.14 = f32[32,64]{1,0:T(8,128)S(1)} all-reduce(f32[32,64]{1,0:T(8,128)S(1)} %bitcast.110), channel_id=1, replica_groups=mesh['gr'=2,'sp'=8,'tp'=2] {'sp'}, use_global_device_ids=true, to_apply=%region_3.4 | all-reduce | flops 2048 | bytes 16384 | tf_op jit(solution)/shard_map/psum | solution.py:126
  211.0 0.6 multiply_reduce_fusion
  211.7 3.1 %psum.15 = f32[]{:T(128)} all-reduce(f32[]{:T(128)} %multiply_reduce_fusion), channel_id=1, replica_groups=mesh['gr'=2,'sp'=8,'tp'=2] {'tp'}, use_global_device_ids=true, to_apply=%region_5.6 | all-reduce | flops 1 | bytes 8 | tf_op jit(solution)/shard_map/psum | solution.py:128
  215.4 0.6 fusion.17
  (48 shorter events, 1.8 us)
Async XLA Ops:
  7.2 14.1 %all-gather.3.cloned.1.call-start = ((), (), s32[]{:S(2)}) async-start(), calls=%async_computation.1 | async-start | bytes 1572864 | tf_op jit(solution)/shard_map/all_gather | solution.py:82
  21.3 2.6 %copy-start.1 = (bf16[256,2048]{1,0:T(8,128)(2,1)S(1)}, bf16[256,2048]{1,0:T(8,128)(2,1)}, u32[]{:S(2)}) copy-start(bf16[256,2048]{1,0:T(8,128)(2,1)} %all-gather.3.cloned.1.call-done) | copy-start | bytes 3145732
  23.9 5.9 %copy-start.5 = (bf16[2048,1024]{1,0:T(8,128)(2,1)S(1)}, bf16[2048,1024]{1,0:T(8,128)(2,1)}, u32[]{:S(2)}) copy-start(bf16[2048,1024]{1,0:T(8,128)(2,1)} %param.14) | copy-start | bytes 12582916
  31.1 5.1 %collective-permute-start = (bf16[2,3072]{1,0:T(2,128)(2,1)S(1)}, bf16[2,3072]{1,0:T(2,128)(2,1)S(1)}, u32[]{:S(2)}, u32[]{:S(2)}) collective-permute-start(bf16[2,3072]{1,0:T(2,128)(2,1)S(1)} %get-tuple-element.6), channel_id=1, source_target_pairs={{0,2},{2,4},{4,6},{6,8},{8,10},{10,12},{12,14},{1,3},{3,5},{5,7},{... | collective-permute-start | bytes 36872 | tf_op jit(solution)/shard_map/ppermute | solution.py:24
  34.8 5.6 %collective-permute-start.1 = (bf16[2,3072]{1,0:T(2,128)(2,1)S(1)}, bf16[2,3072]{1,0:T(2,128)(2,1)S(1)}, u32[]{:S(2)}, u32[]{:S(2)}) collective-permute-start(bf16[2,3072]{1,0:T(2,128)(2,1)S(1)} %get-tuple-element.7), channel_id=1, source_target_pairs={{2,0},{4,2},{6,4},{8,6},{10,8},{12,10},{14,12},{3,1},{5,3},{7,5},{... | collective-permute-start | bytes 36872 | tf_op jit(solution)/shard_map/ppermute | solution.py:25
  78.8 6.3 %copy-start.4 = (bf16[1,8,128]{2,1,0:T(8,128)(2,1)S(1)}, bf16[1,8,128]{2,1,0:T(8,128)(2,1)}, u32[]{:S(2)}) copy-start(bf16[1,8,128]{2,1,0:T(8,128)(2,1)} %param.20) | copy-start | bytes 6148
  78.9 72.0 %all-to-all-start = ((bf16[8,2,65536]{2,1,0:T(2,128)(2,1)}), bf16[8,2,65536]{2,1,0:T(2,128)(2,1)S(1)}, u32[]{:S(2)}, u32[]{:S(2)}) async-start(bf16[8,2,65536]{2,1,0:T(2,128)(2,1)} %reshape.153), calls=%async_computation | async-start | bytes 4194304 | tf_op jit(solution)/shard_map/all_to_all | solution.py:118
  157.4 53.7 %copy-start.2 = (bf16[1,32,64]{2,1,0:T(8,128)(2,1)S(1)}, bf16[1,32,64]{2,1,0:T(8,128)(2,1)}, u32[]{:S(2)}) copy-start(bf16[1,32,64]{2,1,0:T(8,128)(2,1)} %param.21) | copy-start | bytes 12292
  175.2 40.9 %copy-start = (bf16[2,2,32,8,1024]{4,2,1,0,3:T(8,128)(2,1)}, bf16[2,2,32,8,1024]{4,2,1,0,3:T(8,128)(2,1)S(1)}, u32[]{:S(2)}) copy-start(bf16[2,2,32,8,1024]{4,2,1,0,3:T(8,128)(2,1)S(1)} %copy.84) | copy-start | bytes 6291460
  175.2 40.2 %copy-start.3 = (f32[32,64]{1,0:T(8,128)S(1)}, f32[32,64]{1,0:T(8,128)}, u32[]{:S(2)}) copy-start(f32[32,64]{1,0:T(8,128)} %param.23) | copy-start | bytes 24580
Sparse Core Ops, SparseCore 0:
  9.5 11.7 all-gather.2
where the time goes:
time: 224 us; the launch traced here: 223 us
  blocking collectives  101 us (45%)
  local copies, waits for them, and re-layouts  61.6 us (28%)
  between operations  15.7 us (7%)
  waiting for transfers between devices  14.6 us (7%)
  matrix products  13.5 us (6%)
  starting transfers between devices  10.6 us (5%)
  other arithmetic  5.54 us (2%)
    all_gather x1, blocking collectives, per_device(): all_logs = lax.all_gather(closing, 'sp', axis=0, tiled=True)  65.2 us
    psum x1, blocking collectives, per_device(): read_total = lax.psum(partial_read, 'sp')  33.1 us
    unnamed x20, local copies, waits for them, and re-layouts  20.1 us
    all_to_all x1, local copies, waits for them, and re-layouts, per_device(): lax.all_to_all(local_rows, 'sp', split_axis=3, concat_axis=0, tiled=True)  17.8 us
    convert_element_type x1, local copies, waits for them, and re-layouts, per_device(): states.reshape(span_count, 2, heads_local, N * P_SIZE).astype(jnp.bfloat16)  14.1 us
    all_gather x1, waiting for transfers between devices, per_device(): slab_piece = lax.all_gather(inputs, 'tp', axis=1, tiled=True)  9.82 us
    another operation x2, local copies, waits for them, and re-layouts  6.77 us
    dot_general x1, matrix products, per_device(): x_part = jnp.dot(slab_piece, x_weight, preferred_element_type=jnp.float32)  5.86 us
  transfers between devices with their start and end apart: 4, of which 2 were waited for; matrix products, arithmetic and copies ran while one was open for 2% of the time, Pallas kernels for 0%

commit v1 on v0

v1 whole, which is shorter than its diff:
```python
import functools

import jax
import jax.numpy as jnp
from jax import lax
from jax.experimental import pallas as pl
from jax.experimental.pallas import tpu as pltpu
from jax.sharding import PartitionSpec as P

H = 64
P_SIZE = 64
G = 16
N = 128
KW = 5
SPAN = 128
EPSILON = 1e-06
PER = H // G
EDGE = 16
ROWS = 16
PITCH = N + 8
LANES = 128
MESH = pl.DeviceIdType.MESH
F32 = jnp.float32
BF16 = jnp.bfloat16


def conv_silu(projected, taps, tokens):
    rounded = projected.astype(BF16).astype(F32)
    total = rounded.shape[0]
    reach = KW // 2
    mixed = None
    for k in range(KW):
        shift = (reach - k) % total
        moved = rounded if shift == 0 else pltpu.roll(rounded, shift, 0)
        term = taps[k : k + 1] * moved[EDGE : EDGE + tokens]
        mixed = term if mixed is None else mixed + term
    return (mixed / (1.0 + jnp.exp(-mixed))).astype(BF16).astype(F32)


def kernel(
    n, width, x, xw, bw, dtw, bias, rate, cx, cb, q, gate, chosen, gain,
    out, fr,
    xext, xwv, bwv, held, stage, wts, reads, qcol, logs, parts, squares,
    sem_w, sem_own, sem_x, sem_halo, sem_c, sem_y, sem_big, sem_self, sem_sq,
):
    s = lax.axis_index("sp")
    c = lax.axis_index("tp")
    tokens, feats = x.shape
    spans = tokens // SPAN
    heads = xw.shape[1] // P_SIZE
    groups = heads // PER
    tile = min(ROWS, heads)
    blocks = heads // tile
    vcols = PER * P_SIZE
    columns = stage.shape[-1]
    lane = lax.broadcasted_iota(jnp.int32, (1, LANES), 1)
    low = lane < P_SIZE

    def peer(k):
        return lax.rem(s + k, n)

    def mate(k):
        return lax.rem(c + k, width)

    def weight_copies(j):
        at_x = pl.ds(pl.multiple_of(j * vcols, vcols), vcols)
        at_b = pl.ds(pl.multiple_of(j * N, N), N)
        return (
            pltpu.make_async_copy(xw.at[:, at_x], xwv.at[:, at_x], sem_w.at[0, j]),
            pltpu.make_async_copy(bw.at[:, at_b], bwv.at[:, at_b], sem_w.at[1, j]),
        )

    for j in range(groups):
        for copy in weight_copies(j):
            copy.start()
    mine = pl.ds(pl.multiple_of(c * feats, feats), feats)
    own = pltpu.make_async_copy(x, xext.at[pl.ds(EDGE, tokens), mine], sem_own)
    own.start()

    barrier = pltpu.get_barrier_semaphore()

    @pl.loop(1, n)
    def _(k):
        pl.semaphore_signal(barrier, inc=1, device_id={"sp": peer(k), "tp": c}, device_id_type=MESH)

    @pl.loop(1, width)
    def _(k):
        pl.semaphore_signal(barrier, inc=1, device_id={"sp": s, "tp": mate(k)}, device_id_type=MESH)

    @pl.when(s > 0)
    def _():
        @pl.loop(1, width)
        def _(k):
            pl.semaphore_signal(
                barrier, inc=1, device_id={"sp": s - 1, "tp": mate(k)}, device_id_type=MESH
            )

    @pl.when(s < n - 1)
    def _():
        @pl.loop(1, width)
        def _(k):
            pl.semaphore_signal(
                barrier, inc=1, device_id={"sp": s + 1, "tp": mate(k)}, device_id_type=MESH
            )

    @pl.when(s == 0)
    def _():
        xext[pl.ds(0, EDGE), :] = jnp.zeros((EDGE, xext.shape[1]), BF16)

    @pl.when(s == n - 1)
    def _():
        xext[pl.ds(EDGE + tokens, EDGE), :] = jnp.zeros((EDGE, xext.shape[1]), BF16)

    sides = lax.min(s, 1) + lax.min(n - 1 - s, 1)
    pl.semaphore_wait(barrier, n - 1 + (width - 1) * (1 + sides))

    def swap(k):
        return pltpu.make_async_remote_copy(
            src_ref=x,
            dst_ref=xext.at[pl.ds(EDGE, tokens), mine],
            send_sem=sem_x.at[0, k],
            recv_sem=sem_x.at[1, k],
            device_id={"sp": s, "tp": mate(k)},
            device_id_type=MESH,
        )

    for k in range(1, width):
        swap(k).start()

    def halo(up, cross):
        slot = width * up + cross
        return pltpu.make_async_remote_copy(
            src_ref=x.at[pl.ds(tokens - EDGE if up else 0, EDGE), :],
            dst_ref=xext.at[pl.ds(0 if up else EDGE + tokens, EDGE), mine],
            send_sem=sem_halo.at[0, slot],
            recv_sem=sem_halo.at[1, slot],
            device_id={"sp": s + 1 if up else s - 1, "tp": mate(cross)},
            device_id_type=MESH,
        )

    @pl.when(s < n - 1)
    def _():
        for k in range(width):
            halo(1, k).start()

    @pl.when(s > 0)
    def _():
        for k in range(width):
            halo(0, k).start()

    turned = jnp.transpose(q[0].astype(F32))
    for g in range(groups):
        qcol[g] = jnp.broadcast_to(turned[:, g : g + 1], (N, LANES))

    own.wait()
    for k in range(1, width):
        swap(k).wait_recv()

    raw = jnp.dot(xext[pl.ds(EDGE, tokens), :], dtw[...], preferred_element_type=F32)
    offset = jnp.concatenate([bias[0:1, :], bias[1:2, :]], axis=1)
    speed = jnp.concatenate([rate[0:1, :], rate[1:2, :]], axis=1)
    raw = raw.astype(BF16).astype(F32) + offset
    step = jnp.maximum(raw, 0.0) + jnp.log1p(jnp.exp(-jnp.abs(raw)))
    decay = -(step * speed) / (tokens * n)
    row = lax.broadcasted_iota(jnp.int32, (SPAN, SPAN), 0)
    col = lax.broadcasted_iota(jnp.int32, (SPAN, SPAN), 1)
    later = jnp.where(col > row, 1.0, 0.0).astype(F32)
    earlier = jnp.where(col < row, 1.0, 0.0).astype(F32)
    local = lax.rem(2 * H - c * heads, 2 * H)
    sub = lax.broadcasted_iota(jnp.int32, (8, LANES), 0)
    closing = jnp.zeros((8, LANES), F32)
    for j in range(spans):
        piece = decay[j * SPAN : (j + 1) * SPAN]
        ahead = jnp.dot(later, piece, precision=lax.Precision.HIGHEST, preferred_element_type=F32)
        behind = jnp.dot(earlier, piece, precision=lax.Precision.HIGHEST, preferred_element_type=F32)
        weight = jnp.exp(jnp.where(low, ahead, behind)) * step[j * SPAN : (j + 1) * SPAN]
        wts[j] = pltpu.roll(weight, local, 1)
        closing = jnp.where(sub == j, jnp.sum(piece, axis=0, keepdims=True), closing)
    logs[s] = closing

    def log_copy(k):
        return pltpu.make_async_remote_copy(
            src_ref=logs.at[s],
            dst_ref=logs.at[s],
            send_sem=sem_c.at[0, k],
            recv_sem=sem_c.at[1, k],
            device_id={"sp": peer(k), "tp": c},
            device_id_type=MESH,
        )

    @pl.loop(1, n)
    def _(k):
        log_copy(k).start()

    @pl.when(s > 0)
    def _():
        for k in range(width):
            halo(1, k).wait_recv()

    @pl.when(s < n - 1)
    def _():
        for k in range(width):
            halo(0, k).wait_recv()

    def one_group(block, i):
        j = block * (tile // PER) + i
        for copy in weight_copies(j):
            copy.wait()
        at_x = pl.ds(pl.multiple_of(j * vcols, vcols), vcols)
        at_b = pl.ds(pl.multiple_of(j * N, N), N)
        rows = xext[...]
        keys = conv_silu(
            jnp.dot(rows, bwv[:, at_b], preferred_element_type=F32), cb[:, at_b].astype(F32), tokens
        )
        values = conv_silu(
            jnp.dot(rows, xwv[:, at_x], preferred_element_type=F32), cx[:, at_x].astype(F32), tokens
        )
        back = lax.rem(LANES - j * PER, LANES)
        for k in range(spans):
            part = slice(k * SPAN, (k + 1) * SPAN)
            turned_keys = jnp.transpose(keys[part]).astype(BF16)
            weight = pltpu.roll(wts[k], back, 1)
            scaled = []
            for h in range(PER):
                pair = values[part, (h // 2) * LANES : (h // 2 + 1) * LANES]
                other = pltpu.roll(pair, P_SIZE, 1)
                doubled = jnp.where(low, pair, other) if h % 2 == 0 else jnp.where(low, other, pair)
                both = jnp.where(low, weight[:, h : h + 1], weight[:, H + h : H + h + 1])
                scaled.append((doubled * both).astype(BF16))
            states = jnp.dot(
                turned_keys, jnp.concatenate(scaled, axis=1), preferred_element_type=F32
            )
            for h in range(PER):
                state = states[:, h * LANES : (h + 1) * LANES]
                held[k, pl.ds(pl.multiple_of((i * PER + h) * PITCH, 8), N), :] = state
                seen = jnp.sum(qcol[j] * state.astype(BF16).astype(F32), axis=0, keepdims=True)
                reads[k, pl.ds(j * PER + h, 1), :] = seen

    def big_copy(block, k):
        at = pl.ds(block * tile, tile)
        return pltpu.make_async_remote_copy(
            src_ref=stage.at[peer(k), :, :, at, :],
            dst_ref=out.at[pl.ds(s * spans, spans), :, at, :],
            send_sem=sem_big.at[0, block, k],
            recv_sem=sem_big.at[1, block, k],
            device_id={"sp": peer(k), "tp": c},
            device_id_type=MESH,
        )

    def self_copy(block):
        at = pl.ds(block * tile, tile)
        return pltpu.make_async_copy(
            stage.at[s, :, :, at, :], out.at[pl.ds(s * spans, spans), :, at, :], sem_self.at[block]
        )

    def lay_out(block, d):
        for k in range(spans):
            for m in range(columns // LANES):
                first = d * (columns // P_SIZE) + 2 * m
                even = held[k, pl.ds(first, tile, stride=PITCH), :]
                odd = held[k, pl.ds(first + 1, tile, stride=PITCH), :]
                at = pl.ds(m * LANES, LANES)
                stage[d, k, 0, pl.ds(block * tile, tile), at] = jnp.where(
                    low, even, pltpu.roll(odd, P_SIZE, 1)
                ).astype(BF16)
                stage[d, k, 1, pl.ds(block * tile, tile), at] = jnp.where(
                    low, pltpu.roll(even, P_SIZE, 1), odd
                ).astype(BF16)

    def part_copy(k):
        return pltpu.make_async_remote_copy(
            src_ref=parts.at[s],
            dst_ref=parts.at[s],
            send_sem=sem_y.at[0, k],
            recv_sem=sem_y.at[1, k],
            device_id={"sp": peer(k), "tp": c},
            device_id_type=MESH,
        )

    def send_read():
        @pl.loop(1, n)
        def _(k):
            log_copy(k).wait_recv()

        every = logs[...]
        index = lax.broadcasted_iota(jnp.int32, every.shape, 0) * spans + lax.broadcasted_iota(
            jnp.int32, every.shape, 1
        )
        real = lax.broadcasted_iota(jnp.int32, every.shape, 1) < spans
        r = chosen[0]
        table = jnp.zeros((8, LANES), F32)
        for k in range(spans):
            j = s * spans + k
            forward = real & (index > j) & (index <= r) & low[None]
            backward = real & (index < j) & (index >= r) & (~low)[None]
            total = jnp.sum(jnp.where(forward | backward, every, 0.0), axis=0)
            total = jnp.sum(total, axis=0, keepdims=True)
            ahead_on = jnp.where(j <= r, 1.0, 0.0)
            behind_on = jnp.where(j >= r, 1.0, 0.0)
            found = jnp.exp(total) * jnp.where(low, ahead_on, behind_on)
            table = jnp.where(sub == k, found, table)
        table = jnp.transpose(pltpu.roll(table, local, 1))
        sums = jnp.zeros((heads, LANES), F32)
        for k in range(spans):
            spread = jnp.where(low, table[0:heads, k : k + 1], table[H : H + heads, k : k + 1])
            sums = sums + spread * reads[k]
        parts[s] = sums

        @pl.loop(1, n)
        def _(k):
            part_copy(k).start()

    for block in range(blocks):

        @pl.loop(0, tile // PER)
        def _(i, block=block):
            one_group(block, i)

        if block == blocks - 1:
            send_read()

        @pl.loop(1, n)
        def _(k, block=block):
            lay_out(block, peer(k))
            big_copy(block, k).start()

        lay_out(block, s)
        self_copy(block).start()

    @pl.loop(1, n)
    def _(k):
        part_copy(k).wait_recv()

    def add_part(i, total):
        return total + parts[i]

    total = lax.fori_loop(1, n, add_part, parts[0])
    total = total + pltpu.roll(total, P_SIZE, 1)
    door = gate[0].astype(F32)
    gated = total[:, :P_SIZE] * (door / (1.0 + jnp.exp(-door)))
    squares[c] = jnp.broadcast_to(jnp.sum(gated * gated, keepdims=True), (8, LANES))

    def square(k):
        return pltpu.make_async_remote_copy(
            src_ref=squares.at[c],
            dst_ref=squares.at[c],
            send_sem=sem_sq.at[0, k],
            recv_sem=sem_sq.at[1, k],
            device_id={"sp": s, "tp": mate(k)},
            device_id_type=MESH,
        )

    for k in range(1, width):
        square(k).start()
    for k in range(1, width):
        square(k).wait_recv()
    mean = jnp.sum(squares[...], axis=0)[0:1, 0:1] / (H * P_SIZE)
    fr[0] = (gated * lax.rsqrt(mean + EPSILON) * gain[...]).astype(BF16)

    for k in range(1, width):
        square(k).wait_send()
    for k in range(1, width):
        swap(k).wait_send()

    @pl.when(s < n - 1)
    def _():
        for k in range(width):
            halo(1, k).wait_send()

    @pl.when(s > 0)
    def _():
        for k in range(width):
            halo(0, k).wait_send()

    @pl.loop(1, n)
    def _(k):
        log_copy(k).wait_send()
        part_copy(k).wait_send()

    for block in range(blocks):
        self_copy(block).wait()

        @pl.loop(1, n)
        def _(k, block=block):
            big_copy(block, k).wait()


def per_device(x, xw, bw, dtw, bias, rate, cx, cb, q, gate, chosen, gain):
    n = lax.axis_size("sp")
    width = lax.axis_size("tp")
    tokens, feats = x.shape
    depth = xw.shape[0]
    spans = tokens // SPAN
    heads = xw.shape[1] // P_SIZE
    groups = heads // PER
    tile = min(ROWS, heads)
    blocks = heads // tile
    columns = N * P_SIZE // n
    vmem = pl.BlockSpec(memory_space=pltpu.VMEM)
    anywhere = pl.BlockSpec(memory_space=pl.ANY)
    dma = pltpu.SemaphoreType.DMA
    return pl.pallas_call(
        functools.partial(kernel, n, width),
        out_shape=(
            jax.ShapeDtypeStruct((spans * n, 2, heads, columns), BF16),
            jax.ShapeDtypeStruct((1, heads, P_SIZE), BF16),
        ),
        in_specs=[vmem, anywhere, anywhere] + [vmem] * 7
        + [pl.BlockSpec(memory_space=pltpu.SMEM), vmem],
        out_specs=(vmem, vmem),
        scratch_shapes=[
            pltpu.VMEM((tokens + 2 * EDGE, depth), BF16),
            pltpu.VMEM(xw.shape, BF16),
            pltpu.VMEM(bw.shape, BF16),
            pltpu.VMEM((spans, tile * PITCH, LANES), F32),
            pltpu.VMEM((n, spans, 2, heads, columns), BF16),
            pltpu.VMEM((spans, SPAN, LANES), F32),
            pltpu.VMEM((spans, heads, LANES), F32),
            pltpu.VMEM((groups, N, LANES), F32),
            pltpu.VMEM((n, 8, LANES), F32),
            pltpu.VMEM((n, heads, LANES), F32),
            pltpu.VMEM((width, 8, LANES), F32),
            dma((2, groups)),
            dma,
            dma((2, width)),
            dma((2, 2 * width)),
            dma((2, n)),
            dma((2, n)),
            dma((2, blocks, n)),
            dma((blocks,)),
            dma((2, width)),
        ],
        compiler_params=pltpu.CompilerParams(
            collective_id=0, has_side_effects=True, vmem_limit_bytes=48 * 1024 * 1024
        ),
    )(x, xw, bw, dtw, bias, rate, cx, cb, q, gate, chosen, gain)


def solution(mesh):
    return jax.shard_map(
        per_device,
        mesh=mesh,
        in_specs=(
            P(("gr", "sp"), "tp"),
            P(None, "tp"),
            P(None, "tp"),
            P(),
            P(),
            P(),
            P(None, "tp"),
            P(None, "tp"),
            P("gr", "tp", None),
            P("gr", "tp", None),
            P("gr"),
            P("tp", None),
        ),
        out_specs=(P("gr", None, "tp", "sp"), P("gr", "tp", None)),
        check_vma=False,
    )
```

time: 224 us -> 75 us (0.33)
  the two profiles are of different devices: /device:TPU:0 before, /device:TPU:13 now
where the time goes in v1:
time: 75 us; the launch traced here: 74.5 us
  Pallas kernels  64.3 us (86%)
  local copies, waits for them, and re-layouts  8.92 us (12%)
  between operations  1.31 us (2%)
    pallas_call x1, Pallas kernels, per_device(): pl.pallas_call(functools.partial(kernel, n, width), out_shape=(jax.ShapeD...  64.3 us
    unnamed x20, local copies, waits for them, and re-layouts  8.92 us

profile of v1, /device:TPU:13, one launch (start us, length us, event | category | flops | bytes accessed | tf_op | source)
XLA Modules:
  0.0 74.5 jit_solution(10172328845362905828)
XLA Ops:
  1.3 0.0 copy-start
  1.3 1.0 %copy-done = bf16[256,1024]{1,0:T(8,128)(2,1)S(1)} copy-done((bf16[256,1024]{1,0:T(8,128)(2,1)S(1)}, bf16[256,1024]{1,0:T(8,128)(2,1)}, u32[]{:S(2)}) %copy-start) | copy-done | bytes 524312
  2.3 0.0 copy-start.1
  2.3 1.0 %copy-done.1 = bf16[2048,128]{1,0:T(8,128)(2,1)S(1)} copy-done((bf16[2048,128]{1,0:T(8,128)(2,1)S(1)}, bf16[2048,128]{1,0:T(8,128)(2,1)}, u32[]{:S(2)}) %copy-start.1) | copy-done | bytes 524312
  3.4 0.0 copy-start.2
  3.4 0.8 %copy-done.2 = bf16[5,2048]{1,0:T(8,128)(2,1)S(1)} copy-done((bf16[5,2048]{1,0:T(8,128)(2,1)S(1)}, bf16[5,2048]{1,0:T(8,128)(2,1)}, u32[]{:S(2)}) %copy-start.2) | copy-done | bytes 20504
  4.1 0.0 copy-start.3
  4.1 0.7 copy-done.3
  4.8 0.0 copy-start.4
  4.8 0.7 copy-done.4
  5.6 0.0 copy-start.5
  5.6 0.7 copy-done.5
  6.3 0.0 copy-start.6
  6.3 0.7 copy-done.6
  6.9 0.0 copy-start.7
  6.9 0.7 copy-done.7
  7.6 0.0 copy-start.8
  7.6 0.7 copy-done.8
  8.3 64.3 %shard_map.131 = (bf16[16,2,32,1024]{3,2,1,0:T(8,128)(2,1)S(1)}, bf16[1,32,64]{2,1,0:T(8,128)(2,1)S(1)}) custom-call(bf16[256,1024]{1,0:T(8,128)(2,1)S(1)} %copy-done, bf16[2048,2048]{1,0:T(8,128)(2,1)} %xw.1, bf16[2048,1024]{1,0:T(8,128)(2,1)} %bw.1, bf16[2048,128]{1,0:T(8,128)(2,1)S(1)} %copy-done.1, f32[2,64]{1,0:T(2,128)S(1)} %copy-done.7, ...), custom_call_target="tpu_custom_call" | custom-call | tf_op jit(solution)/shard_map/pallas_call | solution.py:402
  72.6 1.3 %copy.17 = bf16[16,2,32,1024]{3,2,1,0:T(8,128)(2,1)} copy(bf16[16,2,32,1024]{3,2,1,0:T(8,128)(2,1)S(1)} %get-tuple-element.4) | data formatting | bytes 4194304
  73.9 0.6 copy.18
Async XLA Ops:
  1.3 1.0 %copy-start = (bf16[256,1024]{1,0:T(8,128)(2,1)S(1)}, bf16[256,1024]{1,0:T(8,128)(2,1)}, u32[]{:S(2)}) copy-start(bf16[256,1024]{1,0:T(8,128)(2,1)} %x.1) | copy-start | bytes 1572868
  2.3 1.0 %copy-start.1 = (bf16[2048,128]{1,0:T(8,128)(2,1)S(1)}, bf16[2048,128]{1,0:T(8,128)(2,1)}, u32[]{:S(2)}) copy-start(bf16[2048,128]{1,0:T(8,128)(2,1)} %dtw.1) | copy-start | bytes 1572868
  3.4 0.8 %copy-start.2 = (bf16[5,2048]{1,0:T(8,128)(2,1)S(1)}, bf16[5,2048]{1,0:T(8,128)(2,1)}, u32[]{:S(2)}) copy-start(bf16[5,2048]{1,0:T(8,128)(2,1)} %cx.1) | copy-start | bytes 61444
  4.1 0.7 copy-start.3
  4.8 0.7 copy-start.4
  5.6 0.7 copy-start.5
  6.3 0.7 copy-start.6
  6.9 0.7 copy-start.7
  7.6 0.7 copy-start.8

commit v2 on v1

v2 whole, which is shorter than its diff:
```python
import functools

import jax
import jax.numpy as jnp
from jax import lax
from jax.experimental import pallas as pl
from jax.experimental.pallas import tpu as pltpu
from jax.sharding import PartitionSpec as P

H = 64
P_SIZE = 64
G = 16
N = 128
KW = 5
SPAN = 128
EPSILON = 1e-06
PER = H // G
EDGE = 16
ROWS = 8
HALF = N // 2
PITCH = HALF + 8
LANES = 128
MESH = pl.DeviceIdType.MESH
F32 = jnp.float32
BF16 = jnp.bfloat16


def conv_silu(projected, taps, tokens):
    rounded = projected.astype(BF16).astype(F32)
    total = rounded.shape[0]
    reach = KW // 2
    mixed = None
    for k in range(KW):
        shift = (reach - k) % total
        moved = rounded if shift == 0 else pltpu.roll(rounded, shift, 0)
        term = taps[k : k + 1] * moved[EDGE : EDGE + tokens]
        mixed = term if mixed is None else mixed + term
    return (mixed / (1.0 + jnp.exp(-mixed))).astype(BF16).astype(F32)


def kernel(
    n, width, x, xw, bw, dtw_h, bias_h, rate_h, cx_h, cb_h, q_h, gate_h, chosen, gain_h,
    out, fr,
    dtw, bias, rate, cx, cb, q, gate, gain,
    xext, xwv, bwv, held, stage, wts, reads, qcol, logs, parts, squares,
    sem_small, sem_w, sem_own, sem_x, sem_far, sem_pass, sem_halo, sem_c, sem_y, sem_big, sem_self, sem_sq,
):
    s = lax.axis_index("sp")
    c = lax.axis_index("tp")
    tokens, feats = x.shape
    spans = tokens // SPAN
    heads = xw.shape[1] // P_SIZE
    groups = heads // PER
    tile = min(ROWS, heads)
    blocks = heads // tile
    vcols = PER * P_SIZE
    columns = stage.shape[-1]
    lane = lax.broadcasted_iota(jnp.int32, (1, LANES), 1)
    low = lane < P_SIZE

    half = n // 2
    side = s // half
    place = lax.rem(s, half)
    across = lax.rem(s + half, n)
    owners = (s, across)

    def peer(k):
        return lax.rem(s + k, n)

    def near(k):
        return lax.rem(place + k, half)

    def mate(k):
        return lax.rem(c + k, width)

    def weight_copies(j):
        at_x = pl.ds(pl.multiple_of(j * vcols, vcols), vcols)
        at_b = pl.ds(pl.multiple_of(j * N, N), N)
        return (
            pltpu.make_async_copy(xw.at[:, at_x], xwv.at[:, at_x], sem_w.at[0, j]),
            pltpu.make_async_copy(bw.at[:, at_b], bwv.at[:, at_b], sem_w.at[1, j]),
        )

    smalls = [
        pltpu.make_async_copy(a, b, sem_small.at[i])
        for i, (a, b) in enumerate(
            (
                (dtw_h, dtw), (bias_h, bias), (rate_h, rate), (cx_h, cx),
                (cb_h, cb), (q_h, q), (gate_h, gate), (gain_h, gain),
            )
        )
    ]
    mine = pl.ds(pl.multiple_of(c * feats, feats), feats)
    own = pltpu.make_async_copy(x, xext.at[0, pl.ds(EDGE, tokens), mine], sem_own)
    own.start()
    for copy in smalls:
        copy.start()
    for j in range(groups):
        for copy in weight_copies(j):
            copy.start()

    barrier = pltpu.get_barrier_semaphore()

    flat = s * width + c

    @pl.loop(1, n * width)
    def _(k):
        other = lax.rem(flat + k, n * width)
        pl.semaphore_signal(
            barrier,
            inc=1,
            device_id={"sp": other // width, "tp": lax.rem(other, width)},
            device_id_type=MESH,
        )

    for b in range(2):

        @pl.when(owners[b] == 0)
        def _(b=b):
            xext[b, pl.ds(0, EDGE), :] = jnp.zeros((EDGE, xext.shape[2]), BF16)

        @pl.when(owners[b] == n - 1)
        def _(b=b):
            xext[b, pl.ds(EDGE + tokens, EDGE), :] = jnp.zeros((EDGE, xext.shape[2]), BF16)

    pl.semaphore_wait(barrier, n * width - 1)

    def swap(k):
        return pltpu.make_async_remote_copy(
            src_ref=x,
            dst_ref=xext.at[0, pl.ds(EDGE, tokens), mine],
            send_sem=sem_x.at[0, k],
            recv_sem=sem_x.at[1, k],
            device_id={"sp": s, "tp": mate(k)},
            device_id_type=MESH,
        )

    def halo(b, up, cross):
        slot = (b * 2 + up) * width + cross
        target = s + 1 if up else s - 1
        return pltpu.make_async_remote_copy(
            src_ref=x.at[pl.ds(tokens - EDGE if up else 0, EDGE), :],
            dst_ref=xext.at[b, pl.ds(0 if up else EDGE + tokens, EDGE), mine],
            send_sem=sem_halo.at[0, slot],
            recv_sem=sem_halo.at[1, slot],
            device_id={
                "sp": target if b == 0 else lax.rem(target + half, n),
                "tp": mate(cross),
            },
            device_id_type=MESH,
        )

    def far(piece):
        return pltpu.make_async_remote_copy(
            src_ref=x.at[pl.ds(piece * SPAN, SPAN), :],
            dst_ref=xext.at[1, pl.ds(EDGE + piece * SPAN, SPAN), mine],
            send_sem=sem_far.at[0, piece],
            recv_sem=sem_far.at[1, piece],
            device_id={"sp": across, "tp": c},
            device_id_type=MESH,
        )

    def hand_on(piece, k):
        at = xext.at[1, pl.ds(EDGE + piece * SPAN, SPAN), mine]
        return pltpu.make_async_remote_copy(
            src_ref=at,
            dst_ref=at,
            send_sem=sem_pass.at[0, piece, k],
            recv_sem=sem_pass.at[1, piece, k],
            device_id={"sp": s, "tp": mate(k)},
            device_id_type=MESH,
        )

    for k in range(1, width):
        swap(k).start()
    for b in range(2):

        @pl.when(s < n - 1)
        def _(b=b):
            for k in range(width):
                halo(b, 1, k).start()

        @pl.when(s > 0)
        def _(b=b):
            for k in range(width):
                halo(b, 0, k).start()

    for piece in range(spans):
        far(piece).start()

    for copy in smalls:
        copy.wait()

    turned = jnp.transpose(q[0].astype(F32))
    turned = jnp.where(side == 0, turned[:HALF], turned[HALF:])
    for g in range(groups):
        qcol[g] = jnp.broadcast_to(turned[:, g : g + 1], (HALF, LANES))

    own.wait()
    for k in range(1, width):
        swap(k).wait_recv()

    offset = jnp.concatenate([bias[0:1, :], bias[1:2, :]], axis=1)
    speed = jnp.concatenate([rate[0:1, :], rate[1:2, :]], axis=1)
    row = lax.broadcasted_iota(jnp.int32, (SPAN, SPAN), 0)
    col = lax.broadcasted_iota(jnp.int32, (SPAN, SPAN), 1)
    later = jnp.where(col > row, 1.0, 0.0).astype(F32)
    earlier = jnp.where(col < row, 1.0, 0.0).astype(F32)
    local = lax.rem(2 * H - c * heads, 2 * H)
    sub = lax.broadcasted_iota(jnp.int32, (8, LANES), 0)

    def weigh(b):
        raw = jnp.dot(xext[b, pl.ds(EDGE, tokens), :], dtw[...], preferred_element_type=F32)
        raw = raw.astype(BF16).astype(F32) + offset
        step = jnp.maximum(raw, 0.0) + jnp.log1p(jnp.exp(-jnp.abs(raw)))
        decay = -(step * speed) / (tokens * n)
        closing = jnp.zeros((8, LANES), F32)
        for j in range(spans):
            part = slice(j * SPAN, (j + 1) * SPAN)
            ahead = jnp.dot(
                later, decay[part], precision=lax.Precision.HIGHEST, preferred_element_type=F32
            )
            behind = jnp.dot(
                earlier, decay[part], precision=lax.Precision.HIGHEST, preferred_element_type=F32
            )
            weight = jnp.exp(jnp.where(low, ahead, behind)) * step[part]
            wts[b * spans + j] = pltpu.roll(weight, local, 1)
            closing = jnp.where(sub == j, jnp.sum(decay[part], axis=0, keepdims=True), closing)
        return closing

    logs[s] = weigh(0)

    def log_copy(k):
        return pltpu.make_async_remote_copy(
            src_ref=logs.at[s],
            dst_ref=logs.at[s],
            send_sem=sem_c.at[0, k],
            recv_sem=sem_c.at[1, k],
            device_id={"sp": peer(k), "tp": c},
            device_id_type=MESH,
        )

    @pl.loop(1, n)
    def _(k):
        log_copy(k).start()

    def halos_in(b):
        @pl.when(owners[b] > 0)
        def _():
            for k in range(width):
                halo(b, 1, k).wait_recv()

        @pl.when(owners[b] < n - 1)
        def _():
            for k in range(width):
                halo(b, 0, k).wait_recv()

    halos_in(0)

    def one_group(b, block, i):
        j = block * (tile // PER) + i
        if b == 0:
            for copy in weight_copies(j):
                copy.wait()
        at_x = pl.ds(pl.multiple_of(j * vcols, vcols), vcols)
        at_b = pl.ds(pl.multiple_of(j * N, N), N)
        rows = xext[b]
        keys = conv_silu(
            jnp.dot(rows, bwv[:, at_b], preferred_element_type=F32), cb[:, at_b].astype(F32), tokens
        )
        values = conv_silu(
            jnp.dot(rows, xwv[:, at_x], preferred_element_type=F32), cx[:, at_x].astype(F32), tokens
        )
        back = lax.rem(LANES - j * PER, LANES)
        for k in range(spans):
            part = slice(k * SPAN, (k + 1) * SPAN)
            turned_keys = jnp.transpose(keys[part])
            turned_keys = jnp.where(side == 0, turned_keys[:HALF], turned_keys[HALF:]).astype(BF16)
            weight = pltpu.roll(wts[b * spans + k], back, 1)
            scaled = []
            for h in range(PER):
                pair = values[part, (h // 2) * LANES : (h // 2 + 1) * LANES]
                other = pltpu.roll(pair, P_SIZE, 1)
                doubled = jnp.where(low, pair, other) if h % 2 == 0 else jnp.where(low, other, pair)
                both = jnp.where(low, weight[:, h : h + 1], weight[:, H + h : H + h + 1])
                scaled.append((doubled * both).astype(BF16))
            states = jnp.dot(
                turned_keys, jnp.concatenate(scaled, axis=1), preferred_element_type=F32
            )
            for h in range(PER):
                state = states[:, h * LANES : (h + 1) * LANES]
                held[k, pl.ds(pl.multiple_of((i * PER + h) * PITCH, 8), HALF), :] = state
                seen = jnp.sum(qcol[j] * state.astype(BF16).astype(F32), axis=0, keepdims=True)
                reads[b * spans + k, pl.ds(j * PER + h, 1), :] = seen

    def goal(b, block):
        at = pl.ds(pl.multiple_of(block * tile, tile), tile)
        return out.at[pl.ds(owners[b] * spans, spans), :, at, :]

    def big_copy(b, block, k):
        return pltpu.make_async_remote_copy(
            src_ref=stage.at[near(k), b, block],
            dst_ref=goal(b, block),
            send_sem=sem_big.at[0, b, block, k],
            recv_sem=sem_big.at[1, b, block, k],
            device_id={"sp": side * half + near(k), "tp": c},
            device_id_type=MESH,
        )

    def self_copy(b, block):
        return pltpu.make_async_copy(
            stage.at[place, b, block], goal(b, block), sem_self.at[b, block]
        )

    def lay_out(b, block, d):
        for k in range(spans):
            for m in range(columns // LANES):
                first = d * (columns // P_SIZE) + 2 * m
                even = held[k, pl.ds(first, tile, stride=PITCH), :]
                odd = held[k, pl.ds(first + 1, tile, stride=PITCH), :]
                at = pl.ds(m * LANES, LANES)
                stage[d, b, block, k, 0, :, at] = jnp.where(
                    low, even, pltpu.roll(odd, P_SIZE, 1)
                ).astype(BF16)
                stage[d, b, block, k, 1, :, at] = jnp.where(
                    low, pltpu.roll(even, P_SIZE, 1), odd
                ).astype(BF16)

    def part_copy(k):
        return pltpu.make_async_remote_copy(
            src_ref=parts.at[s],
            dst_ref=parts.at[s],
            send_sem=sem_y.at[0, k],
            recv_sem=sem_y.at[1, k],
            device_id={"sp": peer(k), "tp": c},
            device_id_type=MESH,
        )

    def send_read():
        @pl.loop(1, n)
        def _(k):
            log_copy(k).wait_recv()

        every = logs[...]
        index = lax.broadcasted_iota(jnp.int32, every.shape, 0) * spans + lax.broadcasted_iota(
            jnp.int32, every.shape, 1
        )
        real = lax.broadcasted_iota(jnp.int32, every.shape, 1) < spans
        r = chosen[0]
        table = jnp.zeros((8, LANES), F32)
        for k in range(2 * spans):
            j = owners[k // spans] * spans + k % spans
            forward = real & (index > j) & (index <= r) & low[None]
            backward = real & (index < j) & (index >= r) & (~low)[None]
            total = jnp.sum(jnp.where(forward | backward, every, 0.0), axis=0)
            total = jnp.sum(total, axis=0, keepdims=True)
            ahead_on = jnp.where(j <= r, 1.0, 0.0)
            behind_on = jnp.where(j >= r, 1.0, 0.0)
            found = jnp.exp(total) * jnp.where(low, ahead_on, behind_on)
            table = jnp.where(sub == k, found, table)
        table = jnp.transpose(pltpu.roll(table, local, 1))
        sums = jnp.zeros((heads, LANES), F32)
        for k in range(2 * spans):
            spread = jnp.where(low, table[0:heads, k : k + 1], table[H : H + heads, k : k + 1])
            sums = sums + spread * reads[k]
        parts[s] = sums

        @pl.loop(1, n)
        def _(k):
            part_copy(k).start()

    def form(b, block):
        @pl.loop(0, tile // PER)
        def _(i):
            one_group(b, block, i)

    def deliver(b, block):
        @pl.loop(1, half)
        def _(k):
            lay_out(b, block, near(k))
            big_copy(b, block, k).start()

        lay_out(b, block, place)
        self_copy(b, block).start()

    @pl.loop(0, blocks)
    def _(block):
        form(0, block)
        deliver(0, block)

    for piece in range(spans):
        far(piece).wait_recv()
        for k in range(1, width):
            hand_on(piece, k).start()
    halos_in(1)
    for piece in range(spans):
        for k in range(1, width):
            hand_on(piece, k).wait_recv()
    weigh(1)

    @pl.loop(0, blocks - 1)
    def _(block):
        form(1, block)
        deliver(1, block)

    form(1, blocks - 1)
    send_read()
    deliver(1, blocks - 1)

    @pl.loop(1, n)
    def _(k):
        part_copy(k).wait_recv()

    def add_part(i, total):
        return total + parts[i]

    total = lax.fori_loop(1, n, add_part, parts[0])
    total = total + pltpu.roll(total, P_SIZE, 1)
    door = gate[0].astype(F32)
    gated = total[:, :P_SIZE] * (door / (1.0 + jnp.exp(-door)))
    squares[c] = jnp.broadcast_to(jnp.sum(gated * gated, keepdims=True), (8, LANES))

    def square(k):
        return pltpu.make_async_remote_copy(
            src_ref=squares.at[c],
            dst_ref=squares.at[c],
            send_sem=sem_sq.at[0, k],
            recv_sem=sem_sq.at[1, k],
            device_id={"sp": s, "tp": mate(k)},
            device_id_type=MESH,
        )

    for k in range(1, width):
        square(k).start()
    for k in range(1, width):
        square(k).wait_recv()
    mean = jnp.sum(squares[...], axis=0)[0:1, 0:1] / (H * P_SIZE)
    fr[0] = (gated * lax.rsqrt(mean + EPSILON) * gain[...]).astype(BF16)

    for k in range(1, width):
        square(k).wait_send()
    for k in range(1, width):
        swap(k).wait_send()

    for b in range(2):

        @pl.when(s < n - 1)
        def _(b=b):
            for k in range(width):
                halo(b, 1, k).wait_send()

        @pl.when(s > 0)
        def _(b=b):
            for k in range(width):
                halo(b, 0, k).wait_send()

    for piece in range(spans):
        far(piece).wait_send()
        for k in range(1, width):
            hand_on(piece, k).wait_send()

    @pl.loop(1, n)
    def _(k):
        log_copy(k).wait_send()
        part_copy(k).wait_send()

    for b in range(2):

        @pl.loop(0, blocks)
        def _(block, b=b):
            self_copy(b, block).wait()

            @pl.loop(1, half)
            def _(k):
                big_copy(b, block, k).wait()


def per_device(x, xw, bw, dtw, bias, rate, cx, cb, q, gate, chosen, gain):
    n = lax.axis_size("sp")
    width = lax.axis_size("tp")
    tokens, feats = x.shape
    depth = xw.shape[0]
    spans = tokens // SPAN
    heads = xw.shape[1] // P_SIZE
    groups = heads // PER
    tile = min(ROWS, heads)
    blocks = heads // tile
    columns = N * P_SIZE // n
    small = (dtw, bias, rate, cx, cb, q, gate, gain)
    vmem = pl.BlockSpec(memory_space=pltpu.VMEM)
    anywhere = pl.BlockSpec(memory_space=pltpu.HBM)
    dma = pltpu.SemaphoreType.DMA
    return pl.pallas_call(
        functools.partial(kernel, n, width),
        out_shape=(
            jax.ShapeDtypeStruct((spans * n, 2, heads, columns), BF16),
            jax.ShapeDtypeStruct((1, heads, P_SIZE), BF16),
        ),
        in_specs=[anywhere] * 10 + [pl.BlockSpec(memory_space=pltpu.SMEM), anywhere],
        out_specs=(vmem, vmem),
        scratch_shapes=[pltpu.VMEM(a.shape, a.dtype) for a in small]
        + [
            pltpu.VMEM((2, tokens + 2 * EDGE, depth), BF16),
            pltpu.VMEM(xw.shape, BF16),
            pltpu.VMEM(bw.shape, BF16),
            pltpu.VMEM((spans, tile * PITCH, LANES), F32),
            pltpu.VMEM((n // 2, 2, blocks, spans, 2, tile, columns), BF16),
            pltpu.VMEM((2 * spans, SPAN, LANES), F32),
            pltpu.VMEM((2 * spans, heads, LANES), F32),
            pltpu.VMEM((groups, HALF, LANES), F32),
            pltpu.VMEM((n, 8, LANES), F32),
            pltpu.VMEM((n, heads, LANES), F32),
            pltpu.VMEM((width, 8, LANES), F32),
            dma((8,)),
            dma((2, groups)),
            dma,
            dma((2, width)),
            dma((2, spans)),
            dma((2, spans, width)),
            dma((2, 4 * width)),
            dma((2, n)),
            dma((2, n)),
            dma((2, 2, blocks, n // 2)),
            dma((2, blocks)),
            dma((2, width)),
        ],
        compiler_params=pltpu.CompilerParams(
            collective_id=0, has_side_effects=True, vmem_limit_bytes=40 * 1024 * 1024
        ),
    )(x, xw, bw, dtw, bias, rate, cx, cb, q, gate, chosen, gain)


def solution(mesh):
    return jax.shard_map(
        per_device,
        mesh=mesh,
        in_specs=(
            P(("gr", "sp"), "tp"),
            P(None, "tp"),
            P(None, "tp"),
            P(),
            P(),
            P(),
            P(None, "tp"),
            P(None, "tp"),
            P("gr", "tp", None),
            P("gr", "tp", None),
            P("gr"),
            P("tp", None),
        ),
        out_specs=(P("gr", None, "tp", "sp"), P("gr", "tp", None)),
        check_vma=False,
    )
```

time: 75 us -> 72.6 us (0.968)
  the two profiles are of different devices: /device:TPU:13 before, /device:TPU:0 now
where the time goes in v2:
time: 72.6 us; the launch traced here: 72.1 us
  Pallas kernels  59.7 us (82%)
  local copies, waits for them, and re-layouts  11.1 us (15%)
  between operations  1.31 us (2%)
    pallas_call x1, Pallas kernels, per_device(): pl.pallas_call(functools.partial(kernel, n, width), out_shape=(jax.ShapeD...  59.7 us
    unnamed x22, local copies, waits for them, and re-layouts  11.1 us

profile of v2, /device:TPU:0, one launch (start us, length us, event | category | flops | bytes accessed | tf_op | source)
XLA Modules:
  0.0 72.1 jit_solution(12895130994880480784)
XLA Ops:
  1.3 0.0 copy-start
  1.3 2.2 %copy-done = bf16[2048,1024]{1,0:T(8,128)(2,1)S(1)} copy-done((bf16[2048,1024]{1,0:T(8,128)(2,1)S(1)}, bf16[2048,1024]{1,0:T(8,128)(2,1)}, u32[]{:S(2)}) %copy-start) | copy-done | bytes 4194328
  3.5 0.0 copy-start.1
  3.5 1.0 %copy-done.1 = bf16[256,1024]{1,0:T(8,128)(2,1)S(1)} copy-done((bf16[256,1024]{1,0:T(8,128)(2,1)S(1)}, bf16[256,1024]{1,0:T(8,128)(2,1)}, u32[]{:S(2)}) %copy-start.1) | copy-done | bytes 524312
  4.5 0.0 copy-start.2
  4.5 1.0 %copy-done.2 = bf16[2048,128]{1,0:T(8,128)(2,1)S(1)} copy-done((bf16[2048,128]{1,0:T(8,128)(2,1)S(1)}, bf16[2048,128]{1,0:T(8,128)(2,1)}, u32[]{:S(2)}) %copy-start.2) | copy-done | bytes 524312
  5.6 0.0 copy-start.3
  5.6 0.8 %copy-done.3 = bf16[5,2048]{1,0:T(8,128)(2,1)S(1)} copy-done((bf16[5,2048]{1,0:T(8,128)(2,1)S(1)}, bf16[5,2048]{1,0:T(8,128)(2,1)}, u32[]{:S(2)}) %copy-start.3) | copy-done | bytes 20504
  6.3 0.0 copy-start.4
  6.3 0.7 copy-done.4
  7.0 0.0 copy-start.5
  7.0 0.7 copy-done.5
  7.7 0.0 copy-start.6
  7.8 0.7 copy-done.6
  8.4 0.0 copy-start.7
  8.4 0.7 copy-done.7
  9.1 0.0 copy-start.8
  9.1 0.7 copy-done.8
  9.8 0.0 copy-start.9
  9.8 0.7 copy-done.9
  10.5 59.7 %shard_map.131 = (bf16[16,2,32,1024]{3,2,1,0:T(8,128)(2,1)S(1)}, bf16[1,32,64]{2,1,0:T(8,128)(2,1)S(1)}) custom-call(bf16[256,1024]{1,0:T(8,128)(2,1)S(1)} %copy-done.1, bf16[2048,2048]{1,0:T(8,128)(2,1)} %xw.1, bf16[2048,1024]{1,0:T(8,128)(2,1)S(1)} %copy-done, bf16[2048,128]{1,0:T(8,128)(2,1)S(1)} %copy-done.2, f32[2,64]{1,0:T(2,128)S(1)} %copy-done.8, ...), custom_call_target="tpu_custom_call" | custom-call | tf_op jit(solution)/shard_map/pallas_call | solution.py:493
  70.2 1.3 %copy.17 = bf16[16,2,32,1024]{3,2,1,0:T(8,128)(2,1)} copy(bf16[16,2,32,1024]{3,2,1,0:T(8,128)(2,1)S(1)} %get-tuple-element.4) | data formatting | bytes 4194304
  71.5 0.6 copy.18
Async XLA Ops:
  1.3 2.2 %copy-start = (bf16[2048,1024]{1,0:T(8,128)(2,1)S(1)}, bf16[2048,1024]{1,0:T(8,128)(2,1)}, u32[]{:S(2)}) copy-start(bf16[2048,1024]{1,0:T(8,128)(2,1)} %bw.1) | copy-start | bytes 12582916
  3.5 1.0 %copy-start.1 = (bf16[256,1024]{1,0:T(8,128)(2,1)S(1)}, bf16[256,1024]{1,0:T(8,128)(2,1)}, u32[]{:S(2)}) copy-start(bf16[256,1024]{1,0:T(8,128)(2,1)} %x.1) | copy-start | bytes 1572868
  4.5 1.0 %copy-start.2 = (bf16[2048,128]{1,0:T(8,128)(2,1)S(1)}, bf16[2048,128]{1,0:T(8,128)(2,1)}, u32[]{:S(2)}) copy-start(bf16[2048,128]{1,0:T(8,128)(2,1)} %dtw_h.1) | copy-start | bytes 1572868
  5.6 0.8 %copy-start.3 = (bf16[5,2048]{1,0:T(8,128)(2,1)S(1)}, bf16[5,2048]{1,0:T(8,128)(2,1)}, u32[]{:S(2)}) copy-start(bf16[5,2048]{1,0:T(8,128)(2,1)} %cx_h.1) | copy-start | bytes 61444
  6.3 0.7 copy-start.4
  7.0 0.7 copy-start.5
  7.7 0.7 copy-start.6
  8.4 0.7 copy-start.7
  9.1 0.7 copy-start.8
  9.8 0.7 copy-start.9

commit v3 on v2

--- a/solution.py
+++ b/solution.py
@@ -257,20 +257,32 @@
 
     halos_in(0)
 
-    def one_group(b, block, i):
-        j = block * (tile // PER) + i
+    pack = tile // PER
+
+    def form(b, block):
         if b == 0:
-            for copy in weight_copies(j):
-                copy.wait()
-        at_x = pl.ds(pl.multiple_of(j * vcols, vcols), vcols)
-        at_b = pl.ds(pl.multiple_of(j * N, N), N)
+            for i in range(pack):
+                for copy in weight_copies(block * pack + i):
+                    copy.wait()
+        at_x = pl.ds(pl.multiple_of(block * pack * vcols, pack * vcols), pack * vcols)
+        at_b = pl.ds(pl.multiple_of(block * pack * N, pack * N), pack * N)
         rows = xext[b]
-        keys = conv_silu(
+        all_keys = conv_silu(
             jnp.dot(rows, bwv[:, at_b], preferred_element_type=F32), cb[:, at_b].astype(F32), tokens
         )
-        values = conv_silu(
+        all_values = conv_silu(
             jnp.dot(rows, xwv[:, at_x], preferred_element_type=F32), cx[:, at_x].astype(F32), tokens
         )
+        for i in range(pack):
+            one_group(
+                b,
+                block * pack + i,
+                i,
+                all_keys[:, i * N : (i + 1) * N],
+                all_values[:, i * vcols : (i + 1) * vcols],
+            )
+
+    def one_group(b, j, i, keys, values):
         back = lax.rem(LANES - j * PER, LANES)
         for k in range(spans):
             part = slice(k * SPAN, (k + 1) * SPAN)
@@ -289,7 +301,7 @@
             )
             for h in range(PER):
                 state = states[:, h * LANES : (h + 1) * LANES]
-                held[k, pl.ds(pl.multiple_of((i * PER + h) * PITCH, 8), HALF), :] = state
+                held[k, pl.ds((i * PER + h) * PITCH, HALF), :] = state
                 seen = jnp.sum(qcol[j] * state.astype(BF16).astype(F32), axis=0, keepdims=True)
                 reads[b * spans + k, pl.ds(j * PER + h, 1), :] = seen
 
@@ -369,11 +381,6 @@
         def _(k):
             part_copy(k).start()
 
-    def form(b, block):
-        @pl.loop(0, tile // PER)
-        def _(i):
-            one_group(b, block, i)
-
     def deliver(b, block):
         @pl.loop(1, half)
         def _(k):
@@ -488,7 +495,7 @@
     columns = N * P_SIZE // n
     small = (dtw, bias, rate, cx, cb, q, gate, gain)
     vmem = pl.BlockSpec(memory_space=pltpu.VMEM)
-    anywhere = pl.BlockSpec(memory_space=pltpu.HBM)
+    anywhere = pl.BlockSpec(memory_space=pl.ANY)
     dma = pltpu.SemaphoreType.DMA
     return pl.pallas_call(
         functools.partial(kernel, n, width),
@@ -497,7 +504,7 @@
             jax.ShapeDtypeStruct((1, heads, P_SIZE), BF16),
         ),
         in_specs=[anywhere] * 10 + [pl.BlockSpec(memory_space=pltpu.SMEM), anywhere],
-        out_specs=(vmem, vmem),
+        out_specs=(anywhere, vmem),
         scratch_shapes=[pltpu.VMEM(a.shape, a.dtype) for a in small]
         + [
             pltpu.VMEM((2, tokens + 2 * EDGE, depth), BF16),
@@ -525,7 +532,7 @@
             dma((2, width)),
         ],
         compiler_params=pltpu.CompilerParams(
-            collective_id=0, has_side_effects=True, vmem_limit_bytes=40 * 1024 * 1024
+            collective_id=0, has_side_effects=True, vmem_limit_bytes=56 * 1024 * 1024
         ),
     )(x, xw, bw, dtw, bias, rate, cx, cb, q, gate, chosen, gain)
 

time: 72.6 us -> 63 us (0.87)
  local copies, waits for them, and re-layouts: 11.1 us -> 3.79 us
  Pallas kernels: 59.7 us -> 57.7 us
    unnamed x22 -> x4, local copies, waits for them, and re-layouts: 11.1 us -> 3.79 us
    pallas_call x1, Pallas kernels: 59.7 us -> 57.7 us  [per_device(): pl.pallas_call(functools.partial(kernel, n, width), out_shape=(jax.ShapeD...]
where the time goes in v3:
time: 63 us; the launch traced here: 62.8 us
  Pallas kernels  57.7 us (92%)
  local copies, waits for them, and re-layouts  3.79 us (6%)
  between operations  1.3 us (2%)
    pallas_call x1, Pallas kernels, per_device(): pl.pallas_call(functools.partial(kernel, n, width), out_shape=(jax.ShapeD...  57.7 us
    unnamed x4, local copies, waits for them, and re-layouts  3.79 us

profile of v3, /device:TPU:0, one launch (start us, length us, event | category | flops | bytes accessed | tf_op | source)
XLA Modules:
  0.0 62.8 jit_solution(7441976867641915189)
XLA Ops:
  1.3 57.7 %shard_map.131 = (bf16[16,2,32,1024]{3,2,1,0:T(8,128)(2,1)}, bf16[1,32,64]{2,1,0:T(8,128)(2,1)}) custom-call(bf16[256,1024]{1,0:T(8,128)(2,1)} %x.1, bf16[2048,2048]{1,0:T(8,128)(2,1)} %xw.1, bf16[2048,1024]{1,0:T(8,128)(2,1)} %bw.1, bf16[2048,128]{1,0:T(8,128)(2,1)} %dtw_h.1, f32[2,64]{1,0:T(2,128)} %bias_h.1, f32[2,64]{1,0:T(2,128)} %rate_h.1, ...), custom_call_target="tpu_custom_call" | custom-call | tf_op jit(solution)/shard_map/pallas_call | solution.py:500
  59.0 0.0 copy-start
  59.0 3.2 %copy.17 = bf16[16,2,32,1024]{3,2,1,0:T(8,128)(2,1)} copy(bf16[16,2,32,1024]{3,2,1,0:T(8,128)(2,1)} %get-tuple-element.4) | data formatting | bytes 4194304
  62.2 0.0 copy-done
  62.2 0.6 copy.18
Async XLA Ops:
  59.0 3.2 %copy-start = (bf16[1,32,64]{2,1,0:T(8,128)(2,1)S(1)}, bf16[1,32,64]{2,1,0:T(8,128)(2,1)}, u32[]{:S(2)}) copy-start(bf16[1,32,64]{2,1,0:T(8,128)(2,1)} %get-tuple-element.5) | copy-start | bytes 12292
